TPU v7x, 32 devices: a whole 2x2x4 slice. The times are simulated.
32 devices in a mesh: grp: 2 (over y), sp: 4 (over z), tp: 4 (over x, core).
Axes of the slice: x: 2, y: 2, z: 4, core: 2. Of those that a mesh axis runs over, the one named last changes fastest.
Arguments:
- latents: bfloat16 [3072, 4096], P(('grp', 'sp', 'tp')), parts along dimension 0, may hold values from -3 to 3
- conditions: float32 [4, 4096], P('grp', 'sp'), parts along dimension 0, may hold values from -6 to 6
- context: bfloat16 [1024, 4096], P(('grp', 'sp')), parts along dimension 0, may hold values from -6 to 6
- w_shift: bfloat16 [4096, 4096], P('sp', 'tp'), may hold values from -0.09375 to 0.09375
- w_scale: bfloat16 [4096, 4096], P('sp', 'tp'), may hold values from -0.09375 to 0.09375
- w_gate: bfloat16 [4096, 4096], P('sp', 'tp'), may hold values from -0.09375 to 0.09375
- w_qdown: bfloat16 [4096, 1024], P(None, 'tp'), may hold values from -2 to 2
- w_kvdown: bfloat16 [4096, 512], P(None, 'tp'), may hold values from -2 to 2
- w_rope: bfloat16 [4096, 32], replicated, may hold values from -0.09375 to 0.09375
- q_gain: float32 [1024], replicated, may hold values from 1 to 24
- latent_norm_gain: float32 [512], replicated, may hold values from 0.1 to 1.9
- query_up_weight: bfloat16 [1024, 3072], P(None, 'tp'), may hold values from -0.1875 to 0.1875
- key_up_weight: bfloat16 [512, 2048], P(None, 'tp'), may hold values from -0.25 to 0.25
- value_up_weight: bfloat16 [512, 2048], P(None, 'tp'), may hold values from -0.25 to 0.25
- context_bias: float32 [32], P('tp'), may hold values from 0.5 to 2
- w_out: bfloat16 [2048, 4096], P(None, 'tp'), may hold values from -0.5 to 0.5
Outputs:
- mixed: bfloat16 [3072, 4096], P(('grp', 'sp', 'tp')), parts along dimension 0
There are 2 independent parts, one for each index of `grp`. A program takes and returns all parts, laid end to end along the dimension named above; an argument that names none is the same for every part. Nothing has to cross between parts.
All inputs are finite; a program needn't handle non-finite values.
Results may differ from a plain program's by a relative error of at most 0.01345.
The roundings to bfloat16 on the way count: a program that leaves them out, or rounds other values in their place, can miss the bound.
Values may be sent and summed in bfloat16 or wider, within the bound.
A program may use at most 64 MiB of HBM per device.

v0:
```python
import jax
import jax.numpy as jnp
from jax import lax
from jax.sharding import PartitionSpec as P

PLAIN_QK_DIM = 64
ROTARY_DIM = 32
VALUE_DIM = 64
GRID_W = 64


EPSILON = 1e-06
NEGATIVE = -1e30


def layer_modulate(row_block, shift_by, scale_by):
    values = row_block.astype(jnp.float32)
    center = values - jnp.mean(values, axis=-1, keepdims=True)
    spread = jnp.mean(center * center, axis=-1, keepdims=True)
    normed = center * lax.rsqrt(spread + EPSILON)
    return (normed * (1.0 + scale_by) + shift_by).astype(jnp.bfloat16)


def rms_scale(raw_rows, gain_vec):
    values = raw_rows.astype(jnp.float32)
    factor = lax.rsqrt(jnp.mean(values * values, axis=-1, keepdims=True) + EPSILON)
    return (values * factor * gain_vec).astype(jnp.bfloat16)


def axial_turn(values, positions):
    freq_count = values.shape[-1] // 4
    inverse = 10000.0 ** (-jnp.arange(freq_count, dtype=jnp.float32) / freq_count)
    grid_row = (positions // GRID_W).astype(jnp.float32)
    grid_col = (positions % GRID_W).astype(jnp.float32)
    target = (positions.shape[0],) + (1,) * (values.ndim - 2) + (freq_count,)
    pieces = []
    for half_index, coordinate in enumerate((grid_row, grid_col)):
        angles = (coordinate[:, None] * inverse[None, :]).reshape(target)
        cosine = jnp.cos(angles)
        sine_of = jnp.sin(angles)
        segment = values[..., 2 * half_index * freq_count : 2 * (half_index + 1) * freq_count]
        low_half = segment[..., :freq_count]
        high_half = segment[..., freq_count:]
        pieces.append(low_half * cosine - high_half * sine_of)
        pieces.append(low_half * sine_of + high_half * cosine)
    return jnp.concatenate(pieces, axis=-1)


def on_device(
    latents,
    conditions,
    context,
    w_shift,
    w_scale,
    w_gate,
    w_qdown,
    w_kvdown,
    w_rope,
    q_gain,
    latent_norm_gain,
    query_up_weight,
    key_up_weight,
    value_up_weight,
    context_bias,
    w_out,
):
    tp_count = lax.axis_size("tp")
    tp_index = lax.axis_index("tp")
    sp_index = lax.axis_index("sp")
    own_rows = latents.shape[0]
    tok_count = own_rows * tp_count
    ctx_share = context.shape[0] // tp_count
    cond_act = jax.nn.silu(conditions).astype(jnp.bfloat16)
    partial_mod = jnp.concatenate(
        [
            jnp.dot(cond_act, w_shift, preferred_element_type=jnp.float32),
            jnp.dot(cond_act, w_scale, preferred_element_type=jnp.float32),
            jnp.dot(cond_act[0:1], w_gate, preferred_element_type=jnp.float32),
        ],
        axis=0,
    )
    summed = lax.psum(partial_mod, "sp")
    modulation = lax.all_gather(summed, "tp", axis=1, tiled=True)
    ctx_own = lax.dynamic_slice_in_dim(context, tp_index * ctx_share, ctx_share, 0)
    h_lat = layer_modulate(latents, modulation[0], modulation[2])
    h_ctx = layer_modulate(ctx_own, modulation[1], modulation[3])
    h_own = jnp.concatenate([h_lat, h_ctx], axis=0)
    rope_raw = jnp.dot(h_own, w_rope, preferred_element_type=jnp.float32)
    own_pos = sp_index * tok_count + tp_index * own_rows + jnp.arange(own_rows, dtype=jnp.int32)
    kr_lat = axial_turn(rope_raw[:own_rows], own_pos).astype(jnp.bfloat16)
    kr_ctx = rope_raw[own_rows:].astype(jnp.bfloat16)
    arrived = lax.all_gather(h_own, "tp", axis=0, tiled=True)
    projected = jnp.concatenate(
        [
            jnp.dot(arrived, w_qdown, preferred_element_type=jnp.float32),
            jnp.dot(arrived, w_kvdown, preferred_element_type=jnp.float32),
        ],
        axis=1,
    ).astype(jnp.bfloat16)
    q_cols = w_qdown.shape[1]
    grouped = projected.reshape(tp_count, own_rows + ctx_share, projected.shape[1])
    cq_cols = grouped[:, :own_rows, :q_cols].reshape(tok_count, q_cols)
    kvl_cols = grouped[:, :own_rows, q_cols:].reshape(tok_count, w_kvdown.shape[1])
    kvc_cols = grouped[:, own_rows:, q_cols:].reshape(tp_count * ctx_share, w_kvdown.shape[1])
    cq_raw, kvl_raw, kvc_raw, krl_all, krc_all = (
        lax.all_gather(cq_cols, "tp", axis=1, tiled=True),
        lax.all_gather(kvl_cols, "tp", axis=1, tiled=True),
        lax.all_gather(kvc_cols, "tp", axis=1, tiled=True),
        lax.all_gather(kr_lat, "tp", axis=0, tiled=True),
        lax.all_gather(kr_ctx, "tp", axis=0, tiled=True),
    )
    cq_all = rms_scale(cq_raw, q_gain)
    ckv_all = jnp.concatenate(
        [rms_scale(kvl_raw, latent_norm_gain), rms_scale(kvc_raw, latent_norm_gain)], axis=0
    )
    kr_all = jnp.concatenate([krl_all, krc_all], axis=0)
    head_count = query_up_weight.shape[1] // (PLAIN_QK_DIM + ROTARY_DIM)
    q_all = jnp.dot(cq_all, query_up_weight, preferred_element_type=jnp.float32)
    q_all = q_all.reshape(tok_count, head_count, PLAIN_QK_DIM + ROTARY_DIM)
    query_pos = sp_index * tok_count + jnp.arange(tok_count, dtype=jnp.int32)
    queries = jnp.concatenate(
        [q_all[..., :PLAIN_QK_DIM], axial_turn(q_all[..., PLAIN_QK_DIM:], query_pos)], axis=-1
    ).astype(jnp.bfloat16)
    q_nope = queries[..., :PLAIN_QK_DIM]
    q_rope = queries[..., PLAIN_QK_DIM:]
    seg_rows = ckv_all.shape[0]
    is_ctx = (jnp.arange(seg_rows, dtype=jnp.int32) >= tok_count).astype(jnp.float32)
    bias_row = context_bias[None, :, None] * is_ctx[None, None, :]
    score_scale = (PLAIN_QK_DIM + ROTARY_DIM) ** (-0.5)

    def attend_block(running, key_block, value_block, rope_block):
        running_max, running_sum, numerator = running
        scores = jnp.einsum("ihd,jhd->ihj", q_nope, key_block, preferred_element_type=jnp.float32)
        scores = scores + jnp.einsum(
            "ihd,jd->ihj", q_rope, rope_block, preferred_element_type=jnp.float32
        )
        scores = scores * score_scale + bias_row
        new_max = jnp.maximum(running_max, jnp.max(scores, axis=-1))
        rescale = jnp.exp(running_max - new_max)
        exponent = jnp.exp(scores - new_max[..., None])
        running_sum = running_sum * rescale + jnp.sum(exponent, axis=-1)
        numerator = numerator * rescale[..., None] + jnp.einsum(
            "ihj,jhd->ihd",
            exponent.astype(jnp.bfloat16),
            value_block,
            preferred_element_type=jnp.float32,
        )
        return (new_max, running_sum, numerator)

    initial = (
        jnp.full((tok_count, head_count), NEGATIVE, jnp.float32),
        jnp.zeros((tok_count, head_count), jnp.float32),
        jnp.zeros((tok_count, head_count, VALUE_DIM), jnp.float32),
    )

    def expand_latent(key_group):
        latent_rows, rope_block = key_group
        key_block = jnp.dot(latent_rows, key_up_weight, preferred_element_type=jnp.float32).astype(
            jnp.bfloat16
        )
        value_block = jnp.dot(
            latent_rows, value_up_weight, preferred_element_type=jnp.float32
        ).astype(jnp.bfloat16)
        return (
            key_block.reshape(seg_rows, head_count, PLAIN_QK_DIM),
            value_block.reshape(seg_rows, head_count, VALUE_DIM),
            rope_block,
        )

    members = (
        lax.all_gather(ckv_all, "sp", axis=0, tiled=True),
        lax.all_gather(kr_all, "sp", axis=0, tiled=True),
    )
    block_count = members[0].shape[0] // seg_rows
    stacked = tuple(
        (member.reshape((block_count, seg_rows) + member.shape[1:]) for member in members)
    )

    def step_fn(state, key_group):
        key_block, value_block, rope_block = expand_latent(key_group)
        return (attend_block(state, key_block, value_block, rope_block), None)

    result, unused = lax.scan(step_fn, initial, stacked)
    running_max, running_sum, numerator = result
    attended = (
        (numerator / running_sum[..., None])
        .astype(jnp.bfloat16)
        .reshape(tok_count, head_count * VALUE_DIM)
    )
    proj_cols = jnp.dot(
        lax.all_gather(attended, "tp", axis=1, tiled=True),
        w_out,
        preferred_element_type=jnp.float32,
    )
    proj_rows = lax.all_to_all(
        proj_cols.astype(jnp.bfloat16), "tp", split_axis=0, concat_axis=1, tiled=True
    )
    mixed_rows = latents.astype(jnp.float32) + modulation[4] * proj_rows.astype(jnp.float32)
    return mixed_rows.astype(jnp.bfloat16)


def solution(mesh):
    in_specs = (
        P(("grp", "sp", "tp"), None),
        P("grp", "sp"),
        P(("grp", "sp"), None),
        P("sp", "tp"),
        P("sp", "tp"),
        P("sp", "tp"),
        P(None, "tp"),
        P(None, "tp"),
        P(),
        P(),
        P(),
        P(None, "tp"),
        P(None, "tp"),
        P(None, "tp"),
        P("tp"),
        P(None, "tp"),
    )
    out_specs = P(("grp", "sp", "tp"), None)
    return jax.shard_map(
        on_device, mesh=mesh, in_specs=in_specs, out_specs=out_specs, check_vma=False
    )
```

profile of v0, /device:TPU:0, one launch (start us, length us, event | category | flops | bytes accessed | tf_op | source)
XLA Modules:
  0.0 225.4 jit_solution(2736552840774866528)
XLA Ops:
  6.6 1.2 convert_reduce_fusion.1
  7.8 1.4 fusion.45
  9.2 1.3 convert_reduce_fusion
  10.6 1.5 fusion.28
  14.2 20.8 %psum.7 = f32[5,1024]{1,0:T(8,128)S(1)} all-reduce(f32[5,1024]{1,0:T(8,128)S(1)} %pad_maximum_fusion.3), channel_id=1, replica_groups=mesh['grp'=2,'sp'=4,'tp'=4] {'sp'}, use_global_device_ids=true, to_apply=%region_0.1 | all-reduce | flops 5120 | bytes 40960 | tf_op jit(solution)/shard_map/psum | solution.py:82
  35.0 5.4 %all_gather.30 = f32[5,4096]{1,0:T(8,128)S(1)} all-gather(f32[5,1024]{1,0:T(8,128)S(1)} %psum.7), channel_id=1, replica_groups=mesh['grp'=2,'sp'=4,'tp'=4] {'tp'}, dimensions={1}, use_global_device_ids=true | all-gather | bytes 102400 | tf_op jit(solution)/shard_map/all_gather | solution.py:83
  40.5 1.1 fusion.48
  42.0 1.1 pad_maximum_fusion
  43.2 32.7 %all-gather.5.cloned.1.call-done = bf16[512,4096]{1,0:T(8,128)(2,1)} async-done(((bf16[128,4096]{1,0:T(8,128)(2,1)}), bf16[512,4096]{1,0:T(8,128)(2,1)}) %all-gather.5.cloned.1.call-update) | async-done | bytes 4194320 | tf_op jit(solution)/shard_map/all_gather | solution.py:92
  75.9 3.7 %convolution_convert_fusion.4 = bf16[512,128]{1,0:T(8,128)(2,1)S(1)} fusion(bf16[512,4096]{1,0:T(8,128)(2,1)} %all-gather.5.cloned.1.call-done, bf16[4096,128]{1,0:T(8,128)(2,1)} %param.25), kind=kOutput, calls=%fused_computation.47 | convolution fusion | flops 536936448 | bytes 5373952 | tf_op jit(solution)/shard_map/dot_general | solution.py:96
  79.7 5.4 %all_gather.33 = bf16[128,512]{1,0:T(8,128)(2,1)S(1)} all-gather(bf16[128,128]{1,0:T(8,128)(2,1)S(1)} %bitcast.114), channel_id=1, replica_groups=mesh['grp'=2,'sp'=4,'tp'=4] {'tp'}, dimensions={1}, use_global_device_ids=true | all-gather | bytes 163840 | tf_op jit(solution)/shard_map/all_gather | solution.py:108
  85.3 6.6 %all_gather.32 = bf16[384,512]{1,0:T(8,128)(2,1)S(1)} all-gather(bf16[384,128]{1,0:T(8,128)(2,1)S(1)} %bitcast.112), channel_id=1, replica_groups=mesh['grp'=2,'sp'=4,'tp'=4] {'tp'}, dimensions={1}, use_global_device_ids=true | all-gather | bytes 491520 | tf_op jit(solution)/shard_map/all_gather | solution.py:107
  93.2 1.7 fusion.82
  95.3 5.2 %all-gather = bf16[4,96,32]{1,2,0:T(8,128)(2,1)S(1)} all-gather(bf16[1,96,32]{1,2,0:T(8,128)(2,1)S(1)} %maximum_bitcast_fusion), channel_id=1, replica_groups=mesh['grp'=2,'sp'=4,'tp'=4] {'tp'}, dimensions={0}, use_global_device_ids=true | all-gather | bytes 30720 | tf_op jit(solution)/shard_map/all_gather | solution.py:109
  100.6 5.2 %all_gather.37 = bf16[128,32]{1,0:T(8,128)(2,1)S(1)} all-gather(bf16[32,32]{1,0:T(8,128)(2,1)S(1)} %copy.33), channel_id=1, replica_groups=mesh['grp'=2,'sp'=4,'tp'=4] {'tp'}, dimensions={0}, use_global_device_ids=true | all-gather | bytes 10240 | tf_op jit(solution)/shard_map/all_gather | solution.py:110
  105.9 14.7 %all_gather.38 = bf16[2048,32]{0,1:T(8,128)(2,1)S(1)} all-gather(bf16[512,32]{0,1:T(8,128)(2,1)S(1)} %pad_maximum_fusion.4), channel_id=1, replica_groups=mesh['grp'=2,'sp'=4,'tp'=4] {'sp'}, dimensions={0}, use_global_device_ids=true | all-gather | bytes 163840 | tf_op jit(solution)/shard_map/all_gather | solution.py:172
  121.4 3.5 %convolution_convert_fusion.3 = bf16[512,256]{1,0:T(8,128)(2,1)S(1)} fusion(bf16[512,4096]{1,0:T(8,128)(2,1)} %all-gather.5.cloned.1.call-done, bf16[4096,256]{1,0:T(8,128)(2,1)S(1)} %copy-done), kind=kOutput, calls=%fused_computation.46 | convolution fusion | flops 1073872896 | bytes 6553600 | tf_op jit(solution)/shard_map/dot_general | solution.py:95
  124.9 7.9 %all_gather.35 = bf16[384,1024]{1,0:T(8,128)(2,1)S(1)} all-gather(bf16[384,256]{1,0:T(8,128)(2,1)S(1)} %bitcast.107), channel_id=1, replica_groups=mesh['grp'=2,'sp'=4,'tp'=4] {'tp'}, dimensions={1}, use_global_device_ids=true | all-gather | bytes 983040 | tf_op jit(solution)/shard_map/all_gather | solution.py:106
  133.1 1.1 fusion.39
  134.4 6.7 %all-gather.7.cloned.1.call-done = bf16[2048,512]{1,0:T(8,128)(2,1)} async-done(((bf16[512,512]{1,0:T(8,128)(2,1)}), bf16[2048,512]{1,0:T(8,128)(2,1)}) %all-gather.7.cloned.1.call-update) | async-done | bytes 2097168 | tf_op jit(solution)/shard_map/all_gather | solution.py:171
  141.1 37.4 %while.15 = (s32[]{:T(128)}, f32[384,8]{0,1:T(8,128)S(1)}, f32[384,8]{0,1:T(8,128)S(1)}, f32[384,8,64]{0,2,1:T(8,128)S(1)}, bf16[4,512,512]{2,1,0:T(8,128)(2,1)}...) while((s32[]{:T(128)}, f32[384,8]{0,1:T(8,128)S(1)}, ...), condition=%wide.region_11.12_spmd.clone, body=%wide.region_8.11_spmd.clone.sunk | while | flops 1053903872 | bytes 38078656 | solution.py:183
  141.2 1.7 convolution_convert_fusion.8
  142.9 1.7 convolution_convert_fusion.7
  144.5 1.8 fusion.128
  146.3 1.9 fusion.129
  148.3 0.8 fusion.130
  149.1 1.3 fusion.132
  150.5 1.7 convolution_convert_fusion.8
  152.2 1.7 convolution_convert_fusion.7
  153.9 1.8 fusion.128
  155.7 1.9 fusion.129
  157.6 0.8 fusion.130
  158.5 1.3 fusion.132
  159.9 1.7 convolution_convert_fusion.8
  161.6 1.7 convolution_convert_fusion.7
  163.3 1.8 fusion.128
  165.1 1.9 fusion.129
  167.9 1.3 fusion.132
  169.3 1.7 convolution_convert_fusion.8
  171.0 1.7 convolution_convert_fusion.7
  172.7 1.8 fusion.128
  174.4 1.9 fusion.129
  177.2 1.3 fusion.132
  179.4 18.6 %all-gather.9.cloned.1.call-done = bf16[384,2048]{0,1:T(8,128)(2,1)} async-done(((bf16[384,512]{0,1:T(8,128)(2,1)}), bf16[384,2048]{0,1:T(8,128)(2,1)}) %all-gather.9.cloned.1.call-update) | async-done | bytes 1572880 | tf_op jit(solution)/shard_map/all_gather | solution.py:191
  198.0 4.5 %convolution_convert_fusion.2 = bf16[384,1024]{1,0:T(8,128)(2,1)S(1)} fusion(bf16[384,2048]{0,1:T(8,128)(2,1)} %all-gather.9.cloned.1.call-done, bf16[2048,1024]{1,0:T(8,128)(2,1)} %param.33), kind=kOutput, calls=%fused_computation.45 | convolution fusion | flops 1611005952 | bytes 6553600 | tf_op jit(solution)/shard_map/dot_general | solution.py:190
  202.5 14.0 %all_to_all.13 = bf16[4,96,1024]{2,1,0:T(8,128)(2,1)S(1)} all-to-all(bf16[4,96,1024]{2,1,0:T(8,128)(2,1)S(1)} %bitcast.106), channel_id=1, replica_groups=mesh['grp'=2,'sp'=4,'tp'=4] {'tp'}, dimensions={0} | all-to-all | bytes 1572864 | tf_op jit(solution)/shard_map/all_to_all | solution.py:195
  216.9 1.0 copy-done.2
  217.8 1.1 fusion.35
  (91 shorter events, 9.0 us)
Async XLA Ops:
  6.5 114.9 %copy-start = (bf16[4096,256]{1,0:T(8,128)(2,1)S(1)}, bf16[4096,256]{1,0:T(8,128)(2,1)}, u32[]{:S(2)}) copy-start(bf16[4096,256]{1,0:T(8,128)(2,1)} %param.24) | copy-start | bytes 6291460
  6.5 5.6 %copy-start.8 = (f32[2,1024]{1,0:T(2,128)S(1)}, f32[2,1024]{1,0:T(2,128)}, u32[]{:S(2)}) copy-start(f32[2,1024]{1,0:T(2,128)} %param.19) | copy-start | bytes 24580
  6.5 69.4 %all-gather.5.cloned.1.call-start = ((), (), s32[]{:S(2)}) async-start(), calls=%async_computation.1 | async-start | bytes 5242880 | tf_op jit(solution)/shard_map/all_gather | solution.py:92
  6.5 5.6 %copy-start.3 = (bf16[1024,1024]{1,0:T(8,128)(2,1)S(1)}, bf16[1024,1024]{1,0:T(8,128)(2,1)}, u32[]{:S(2)}) copy-start(bf16[1024,1024]{1,0:T(8,128)(2,1)} %param.23) | copy-start | bytes 6291460
  6.5 6.0 %copy-start.4 = (bf16[1024,1024]{1,0:T(8,128)(2,1)S(1)}, bf16[1024,1024]{1,0:T(8,128)(2,1)}, u32[]{:S(2)}) copy-start(bf16[1024,1024]{1,0:T(8,128)(2,1)} %param.22) | copy-start | bytes 6291460
  12.2 1.6 copy-start.5
  12.6 29.0 %copy-start.1 = (bf16[96,4096]{1,0:T(8,128)(2,1)S(1)}, bf16[96,4096]{1,0:T(8,128)(2,1)}, u32[]{:S(2)}) copy-start(bf16[96,4096]{1,0:T(8,128)(2,1)} %param.18) | copy-start | bytes 2359300
  43.1 98.0 %all-gather.7.cloned.1.call-start = ((), (), s32[]{:S(2)}) async-start(), calls=%async_computation.2 | async-start | bytes 2621440 | tf_op jit(solution)/shard_map/all_gather | solution.py:171
  43.2 48.9 %copy-start.7 = (f32[512]{0:T(512)S(1)}, f32[512]{0:T(512)}, u32[]{:S(2)}) copy-start(f32[512]{0:T(512)} %param.28) | copy-start | bytes 6148
  93.2 104.8 %all-gather.9.cloned.1.call-start = ((), (), s32[]{:S(2)}) async-start(), calls=%async_computation.3 | async-start | bytes 1966080 | tf_op jit(solution)/shard_map/all_gather | solution.py:191
  124.9 8.2 %copy-start.9 = (bf16[1024,768]{1,0:T(8,128)(2,1)S(1)}, bf16[1024,768]{1,0:T(8,128)(2,1)}, u32[]{:S(2)}) copy-start(bf16[1024,768]{1,0:T(8,128)(2,1)} %param.29) | copy-start | bytes 4718596
  124.9 8.2 %copy-start.10 = (f32[1024]{0:T(1024)S(1)}, f32[1024]{0:T(1024)}, u32[]{:S(2)}) copy-start(f32[1024]{0:T(1024)} %param.27) | copy-start | bytes 12292
  133.1 8.0 %copy-start.6 = (f32[8]{0:T(128)S(1)}, f32[8]{0:T(128)}, u32[]{:S(2)}) copy-start(f32[8]{0:T(128)} %param.32) | copy-start | bytes 100
  216.7 1.1 copy-start.2
Sparse Core Ops, SparseCore 0:
  43.2 32.6 all-gather.4
  93.3 47.7 all-gather.6
  179.5 18.4 all-gather.8
where the time goes:
time: 226 us; the launch traced here: 225 us
  blocking collectives  85.3 us (38%)
  waiting for transfers between devices  58.1 us (26%)
  matrix products  49 us (22%)
  other arithmetic  16.1 us (7%)
  between operations  13.5 us (6%)
  local copies, waits for them, and re-layouts  3.08 us (1%)
    all_gather x1, waiting for transfers between devices, on_device(): arrived = lax.all_gather(h_own, 'tp', axis=0, tiled=True)  32.7 us
    psum x1, blocking collectives, on_device(): summed = lax.psum(partial_mod, 'sp')  20.8 us
    all_gather x1, waiting for transfers between devices, on_device(): lax.all_gather(attended, 'tp', axis=1, tiled=True)  18.6 us
    all_gather x1, blocking collectives, on_device(): lax.all_gather(kr_all, 'sp', axis=0, tiled=True)  14.7 us
    all_to_all x1, blocking collectives, on_device(): lax.all_to_all(proj_cols.astype(jnp.bfloat16), 'tp', split_axis=0, concat...  14 us
    all_gather x1, blocking collectives, on_device(): lax.all_gather(cq_cols, 'tp', axis=1, tiled=True)  7.9 us
    dot_general x4, matrix products, attend_block(): jnp.einsum('ihd,jhd->ihj', q_nope, key_block, preferred_element_type=jnp....  7.78 us
    dot_general x4, matrix products, attend_block(): jnp.einsum('ihd,jd->ihj', q_rope, rope_block, preferred_element_type=jnp....  7.05 us
  transfers between devices with their start and end apart: 3, of which 3 were waited for; matrix products, arithmetic and copies ran while one was open for 4% of the time, Pallas kernels for 0%

commit v1 on v0

--- a/solution.py
+++ b/solution.py
@@ -1,6 +1,11 @@
+import functools
+
 import jax
 import jax.numpy as jnp
+import numpy as np
 from jax import lax
+from jax.experimental import pallas as pl
+from jax.experimental.pallas import tpu as pltpu
 from jax.sharding import PartitionSpec as P
 
 PLAIN_QK_DIM = 64
@@ -46,7 +51,7 @@
     return jnp.concatenate(pieces, axis=-1)
 
 
-def on_device(
+def plain_device(
     latents,
     conditions,
     context,
@@ -199,6 +204,655 @@
     return mixed_rows.astype(jnp.bfloat16)
 
 
+MESH = pl.DeviceIdType.MESH
+LOG2E = 1.4426950408889634
+STEP = 16
+
+
+def turn_tables(tokens):
+    freq_count = ROTARY_DIM // 4
+    inverse = 10000.0 ** (-np.arange(freq_count) / freq_count)
+    position = np.arange(tokens)
+    cosine = np.zeros((tokens, 128), np.float32)
+    sine = np.zeros((tokens, 128), np.float32)
+    cosine[:, :PLAIN_QK_DIM] = 1.0
+    for half_index, coordinate in enumerate((position // GRID_W, position % GRID_W)):
+        angles = coordinate[:, None] * inverse[None, :]
+        low = PLAIN_QK_DIM + 2 * half_index * freq_count
+        high = low + freq_count
+        cosine[:, low : low + freq_count] = np.cos(angles)
+        cosine[:, high : high + freq_count] = np.cos(angles)
+        sine[:, low : low + freq_count] = -np.sin(angles)
+        sine[:, high : high + freq_count] = np.sin(angles)
+    return cosine, sine
+
+
+def lanes_of(shape):
+    return lax.broadcasted_iota(jnp.int32, shape, len(shape) - 1)
+
+
+def turned(values, cosine, sine):
+    lane = lanes_of(values.shape)
+    swapped = jnp.where(
+        (lane // 8) % 2 == 0, pltpu.roll(values, 120, 1), pltpu.roll(values, 8, 1)
+    )
+    return values * cosine + swapped * sine
+
+
+def block_kernel(
+    cond_ref,
+    bias_ref,
+    qgain_ref,
+    kvgain_ref,
+    rope_ref,
+    lat_hbm,
+    ctx_hbm,
+    wsh_hbm,
+    wsc_hbm,
+    wga_hbm,
+    wqd_hbm,
+    wkd_hbm,
+    wqu_hbm,
+    wku_hbm,
+    wvu_hbm,
+    wo_hbm,
+    cos_hbm,
+    sin_hbm,
+    out_ref,
+    cond16,
+    w3,
+    lat,
+    ctx,
+    hid,
+    wqd,
+    wkvr,
+    modp,
+    mod,
+    cq,
+    kv,
+    kvc,
+    kraw,
+    ck,
+    cqn,
+    wqu,
+    wku,
+    wvu,
+    wo,
+    cosv,
+    sinv,
+    qh,
+    kb,
+    vb,
+    acc,
+    mx,
+    att,
+    po,
+    pr,
+    load_sem,
+    send_sem,
+    recv_sem,
+    zsend,
+    zrecv,
+    dsend,
+    drecv,
+):
+    f32, bf16 = jnp.float32, jnp.bfloat16
+    spn = lax.axis_size("sp")
+    p = lax.axis_index("tp")
+    z = lax.axis_index("sp")
+    core = lax.rem(p, 2)
+    side = p // 2
+    p1, p2, p3 = p ^ 1, p ^ 2, p ^ 3
+    own = lat.shape[1]
+    width = lat.shape[2]
+    tok = own * 4
+    pair = own * 2
+    ctxn = ctx.shape[0]
+    seg = tok + ctxn
+    modw = w3.shape[2]
+    heads = qh.shape[0]
+    hrow = seg // 2
+    qcols = cq.shape[3]
+    kcols = kv.shape[3]
+    krank = 4 * kcols
+
+    loads = []
+
+    def load(src, dst):
+        copy = pltpu.make_async_copy(src, dst, load_sem.at[len(loads)])
+        loads.append(copy)
+        copy.start()
+        return copy
+
+    l_lat = load(lat_hbm, lat.at[p])
+    l_w3 = [load(ref, w3.at[i]) for i, ref in enumerate((wsh_hbm, wsc_hbm, wga_hbm))]
+    l_ctx = load(ctx_hbm, ctx)
+    l_kd = load(wkd_hbm, wkvr.at[:, pl.ds(0, kcols)])
+    l_qd = load(wqd_hbm, wqd)
+    table_rows = pl.ds(pl.multiple_of(z * tok, 8), tok)
+    l_cos = load(cos_hbm.at[table_rows], cosv)
+    l_sin = load(sin_hbm.at[table_rows], sinv)
+    l_ku = load(wku_hbm, wku)
+    l_vu = load(wvu_hbm, wvu)
+    l_qu = load(wqu_hbm, wqu)
+    l_wo = load(wo_hbm, wo)
+
+    barrier = pltpu.get_barrier_semaphore()
+    for peer in (p1, p2, p3):
+        pl.semaphore_signal(barrier, inc=1, device_id={"tp": peer}, device_id_type=MESH)
+    for d in range(1, spn):
+        pl.semaphore_signal(
+            barrier, inc=1, device_id={"sp": lax.rem(z + d, spn)}, device_id_type=MESH
+        )
+
+    sends = []
+
+    def remote(src, dst, index, target):
+        return pltpu.make_async_remote_copy(
+            src_ref=src,
+            dst_ref=dst,
+            send_sem=send_sem.at[index],
+            recv_sem=recv_sem.at[index],
+            device_id=target,
+            device_id_type=MESH,
+        )
+
+    def send(src, dst, index, target):
+        copy = remote(src, dst, index, target)
+        copy.start()
+        sends.append(copy)
+        return copy
+
+    counter = [0]
+
+    def fresh():
+        counter[0] += 1
+        return counter[0] - 1
+
+    def spread(view, far_view=None):
+        far_view = far_view or view
+        i1, i2, i3 = fresh(), fresh(), fresh()
+        first = send(view(p), view(p), i2, {"tp": p2})
+        second = send(view(p), view(p), i1, {"tp": p1})
+
+        def relay():
+            first.wait_recv()
+            third = send(far_view(p2), far_view(p2), i3, {"tp": p1})
+            return third.wait_recv
+
+        return relay, second.wait_recv
+
+    cond16[...] = jnp.zeros_like(cond16)
+    cond16[0:2, :] = cond_ref[...]
+    conditions = cond16[...]
+    act = (conditions / (1.0 + jnp.exp(-conditions))).astype(bf16)
+
+    pl.semaphore_wait(barrier, 3 + spn - 1)
+    l_lat.wait()
+    half_own = own // 2
+    relay_lat = []
+    lat_near = []
+    for piece in range(2):
+        rows = pl.ds(piece * half_own, half_own)
+        r, w = spread(lambda slot, rows=rows: lat.at[slot, rows])
+        relay_lat.append(r)
+        lat_near.append(w)
+
+    for i in range(3):
+        l_w3[i].wait()
+        part = jnp.dot(act, w3[i], preferred_element_type=f32)
+        modp[z, 2 * i : 2 * i + 2, :] = part[0:2]
+    modp[z, 6:8, :] = jnp.zeros((2, modw), f32)
+    mod_waits = []
+    for d in range(1, spn):
+        mod_waits.append(
+            send(modp.at[z], modp.at[z], fresh(), {"sp": lax.rem(z + d, spn)})
+        )
+    wkvr[:, kcols:] = jnp.zeros((width, wkvr.shape[1] - kcols), bf16)
+    wkvr[:, kcols : kcols + ROTARY_DIM] = rope_ref[...]
+    for copy in mod_waits:
+        copy.wait_recv()
+    total = modp[0]
+    for i in range(1, spn):
+        total = total + modp[i]
+    mod[p] = total
+    mod_waits = [send(mod.at[p], mod.at[p], fresh(), {"tp": peer}) for peer in (p2, p3, p1)]
+    lat_far = [relay_lat[0]()]
+    for copy in mod_waits:
+        copy.wait_recv()
+
+    def modulate(src, row_count, dst_row, which):
+        @pl.loop(0, row_count // STEP)
+        def _(i):
+            rows = pl.ds(pl.multiple_of(i * STEP, STEP), STEP)
+            values = src[rows, :].astype(f32)
+            center = values - jnp.mean(values, axis=-1, keepdims=True)
+            spread_of = jnp.mean(center * center, axis=-1, keepdims=True)
+            normed = center * lax.rsqrt(spread_of + EPSILON)
+            to = pl.ds(pl.multiple_of(dst_row + i * STEP, STEP), STEP)
+            for j in range(4):
+                shift_by = mod[j, which : which + 1, :]
+                scale_by = mod[j, 2 + which : 3 + which, :]
+                cols = slice(j * modw, (j + 1) * modw)
+                hid[to, cols] = (normed[:, cols] * (1.0 + scale_by) + shift_by).astype(bf16)
+
+    l_ctx.wait()
+    modulate(ctx, ctxn, tok, 1)
+    l_kd.wait()
+    l_qd.wait()
+    mixed_ctx = jnp.dot(hid[tok:, :], wkvr[...], preferred_element_type=f32)
+    kvc[p] = mixed_ctx[:, :kcols].astype(bf16)
+    kraw[tok:, :] = mixed_ctx[:, kcols:]
+    relays = [spread(lambda slot: kvc.at[slot])]
+
+    modulate(lat.at[p], own, p * own, 0)
+    for w in lat_near:
+        w()
+    modulate(lat.at[p1], own, p1 * own, 0)
+
+    def down(half):
+        rows = pl.ds(pl.multiple_of(half * pair, STEP), pair)
+        both = jnp.dot(hid[rows, :], wkvr[...], preferred_element_type=f32)
+        kv[p, half] = both[:, :kcols].astype(bf16)
+        kraw[rows, :] = both[:, kcols:]
+        one = spread(lambda slot: kv.at[slot, half], lambda slot: kv.at[slot, 1 - half])
+        cq[p, half] = jnp.dot(hid[rows, :], wqd[...], preferred_element_type=f32).astype(bf16)
+        return one, spread(lambda slot: cq.at[slot, half], lambda slot: cq.at[slot, 1 - half])
+
+    kv_a, cq_a = down(side)
+    lat_far.append(relay_lat[1]())
+    modulate(lat.at[p2], own, p2 * own, 0)
+    for w in lat_far:
+        w()
+    modulate(lat.at[p3], own, p3 * own, 0)
+    kv_b, cq_b = down(1 - side)
+    relays += [kv_a, kv_b]
+    far = [r() for r, _ in relays]
+    for w in far:
+        w()
+    for _, near in relays:
+        near()
+
+    l_cos.wait()
+    l_sin.wait()
+    kr_lat = turned(pltpu.roll(kraw[:tok, :], 64, 1), cosv[...], sinv[...])
+    kraw[:tok, :] = kr_lat
+    kraw[tok:, :] = pltpu.roll(kraw[tok:, :], 64, 1)
+    for hf in range(2):
+        for t in range(4):
+            packed = None
+            for j in range(4):
+                first_row = hf * hrow + (4 * t + j) * STEP
+                moved = pltpu.roll(
+                    kraw[first_row : first_row + STEP, :], (32 * j + 64) % 128, 1
+                )
+                packed = moved if packed is None else packed + moved
+            ck[z, hf, hrow : hrow + STEP, 128 * t : 128 * t + 128] = packed.astype(bf16)
+
+    def rms(pieces, gain_ref, store):
+        values = [piece.astype(f32) for piece in pieces]
+        total_of = None
+        for v in values:
+            s = jnp.sum(v * v, axis=-1, keepdims=True)
+            total_of = s if total_of is None else total_of + s
+        cols = values[0].shape[1]
+        factor = lax.rsqrt(total_of / (cols * len(values)) + EPSILON)
+        for j, v in enumerate(values):
+            gain = gain_ref[0:1, j * cols : (j + 1) * cols]
+            store(slice(j * cols, (j + 1) * cols), (v * factor * gain).astype(bf16))
+
+    for piece in range(seg // 64):
+        base = piece * 64
+        if base < tok:
+            chunk = [kv[r, base // pair, base % pair : base % pair + 64, :] for r in range(4)]
+        else:
+            chunk = [kvc[r, base - tok : base - tok + 64, :] for r in range(4)]
+
+        def put(cols, value, base=base):
+            ck[z, base // hrow, base % hrow : base % hrow + 64, cols] = value
+
+        rms(chunk, kvgain_ref, put)
+
+    def hop(origin, target, way):
+        return pltpu.make_async_remote_copy(
+            src_ref=ck.at[origin, core],
+            dst_ref=ck.at[origin, core],
+            send_sem=zsend.at[way, origin],
+            recv_sem=zrecv.at[origin],
+            device_id={"sp": target},
+            device_id_type=MESH,
+        )
+
+    def cross(origin, half):
+        return pltpu.make_async_remote_copy(
+            src_ref=ck.at[origin, half],
+            dst_ref=ck.at[origin, half],
+            send_sem=dsend.at[origin],
+            recv_sem=drecv.at[origin],
+            device_id={"tp": p1},
+            device_id_type=MESH,
+        )
+
+    has_right = z + 1 < spn
+    has_left = z >= 1
+
+    @pl.when(has_right)
+    def _():
+        hop(z, z + 1, 0).start()
+
+    @pl.when(has_left)
+    def _():
+        hop(z, z - 1, 1).start()
+
+    w_cq = [cq_a[0](), cq_b[0]()]
+    for w in w_cq:
+        w()
+    cq_a[1]()
+    cq_b[1]()
+    for piece in range(tok // 64):
+        base = piece * 64
+        chunk = [cq[r, base // pair, base % pair : base % pair + 64, :] for r in range(4)]
+
+        def put(cols, value, base=base):
+            cqn[base : base + 64, cols] = value
+
+        rms(chunk, qgain_ref, put)
+    l_qu.wait()
+    q_all = jnp.dot(cqn[...], wqu[...], preferred_element_type=f32)
+    lane = lanes_of((tok, 128))
+    for h in range(heads):
+        offset = h * (PLAIN_QK_DIM + ROTARY_DIM)
+        tile, shift = offset // 128, offset % 128
+        head = q_all[:, 128 * tile : 128 * tile + 128]
+        if shift:
+            head = pltpu.roll(head, 128 - shift, 1)
+            if shift + PLAIN_QK_DIM + ROTARY_DIM > 128:
+                rest = pltpu.roll(q_all[:, 128 * tile + 128 : 128 * tile + 256], 128 - shift, 1)
+                head = jnp.where(lane < 128 - shift, head, rest)
+        qh[h] = turned(head, cosv[...], sinv[...]).astype(bf16)
+    l_ku.wait()
+    l_vu.wait()
+    acc[...] = jnp.zeros_like(acc)
+    mx[...] = jnp.full(mx.shape, NEGATIVE, f32)
+    factor = (PLAIN_QK_DIM + ROTARY_DIM) ** (-0.5) * LOG2E
+
+    def arrive(step):
+        left, right = z - 1 - step, z + 1 + step
+
+        @pl.when(left >= 0)
+        def _():
+            hop(left, z, 0).wait_recv()
+            cross(left, core).start()
+
+            @pl.when(has_right)
+            def _():
+                hop(left, z + 1, 0).start()
+
+        @pl.when(right < spn)
+        def _():
+            hop(right, z, 1).wait_recv()
+            cross(right, core).start()
+
+            @pl.when(has_left)
+            def _():
+                hop(right, z - 1, 1).start()
+
+    def expand(block):
+        lane_h = lanes_of((hrow, 128))
+        ones = (lane_h == VALUE_DIM).astype(f32)
+        lane_s = lanes_of((STEP, 128))
+        on_rope = (lane_s >= PLAIN_QK_DIM) & (lane_s < PLAIN_QK_DIM + ROTARY_DIM)
+        for hf in range(2):
+            rows = slice(hf * hrow, (hf + 1) * hrow)
+            latent_rows = ck[block, hf, :hrow, :]
+            pieces = []
+            for t in range(4):
+                packed = ck[block, hf, hrow : hrow + STEP, 128 * t : 128 * t + 128].astype(f32)
+                for j in range(4):
+                    moved = pltpu.roll(packed, (192 - 32 * j) % 128, 1)
+                    pieces.append(jnp.where(on_rope, moved, 0.0))
+            rope_key = jnp.concatenate(pieces, axis=0)
+            keys = jnp.dot(latent_rows, wku[...], preferred_element_type=f32)
+            vals = jnp.dot(latent_rows, wvu[...], preferred_element_type=f32)
+            for hp in range(heads // 2):
+                cols = slice(128 * hp, 128 * hp + 128)
+                k2, v2 = keys[:, cols], vals[:, cols]
+                kb[2 * hp, rows, :] = jnp.where(lane_h < 64, k2, rope_key).astype(bf16)
+                kb[2 * hp + 1, rows, :] = jnp.where(
+                    lane_h < 64, pltpu.roll(k2, 64, 1), rope_key
+                ).astype(bf16)
+                vb[2 * hp, rows, :] = jnp.where(lane_h < 64, v2, ones).astype(bf16)
+                vb[2 * hp + 1, rows, :] = jnp.where(
+                    lane_h < 64, pltpu.roll(v2, 64, 1), ones
+                ).astype(bf16)
+
+    def attend(h):
+        scores = lax.dot_general(
+            qh[h], kb[h], (((1,), (1,)), ((), ())), preferred_element_type=f32
+        )
+        lat_s = scores[:, :tok] * factor
+        ctx_s = scores[:, tok:] * factor + bias_ref[h] * LOG2E
+        old = mx[h]
+        best = jnp.maximum(
+            jnp.max(lat_s, axis=-1, keepdims=True), jnp.max(ctx_s, axis=-1, keepdims=True)
+        )
+        new = jnp.maximum(old, best)
+        mx[h] = new
+        top = new[:, 0:1]
+        weights = jnp.concatenate([jnp.exp2(lat_s - top), jnp.exp2(ctx_s - top)], axis=1)
+        acc[h] = acc[h] * jnp.exp2(old - new) + jnp.dot(
+            weights.astype(bf16), vb[h], preferred_element_type=f32
+        )
+
+    def block_at(step):
+        below = jnp.minimum(z, spn - 1 - z)
+        near = jnp.where(lax.rem(step, 2) == 1, z - (step + 1) // 2, z + step // 2)
+        past = jnp.where(z < spn - 1 - z, step, spn - 1 - step)
+        return jnp.where(step <= 2 * below, near, past)
+
+    @pl.loop(0, spn)
+    def _(step):
+        @pl.when(step > 0)
+        def _():
+            arrive(step - 1)
+
+        block = block_at(step)
+
+        @pl.when(step > 0)
+        def _():
+            cross(block, 1 - core).wait_recv()
+
+        expand(block)
+        for h in range(heads):
+            attend(h)
+
+    att_relays = []
+    lane64 = lane < 64
+    for hp in range(heads // 2):
+        outs = []
+        for h in (2 * hp, 2 * hp + 1):
+            a = acc[h]
+            outs.append(a / a[:, VALUE_DIM : VALUE_DIM + 1])
+        att[p, hp] = jnp.where(lane64, outs[0], pltpu.roll(outs[1], 64, 1)).astype(bf16)
+        att_relays.append(spread(lambda slot, hp=hp: att.at[slot, hp]))
+    att_far = [r() for r, _ in att_relays]
+    for w in att_far:
+        w()
+    for _, near in att_relays:
+        near()
+    l_wo.wait()
+    final = []
+    for dest in (p2, p3, p1, p):
+        rows = pl.ds(pl.multiple_of(dest * own, STEP), own)
+        joined = jnp.concatenate(
+            [att[r, hp, rows, :] for r in range(4) for hp in range(heads // 2)], axis=1
+        )
+        made = jnp.dot(joined, wo[...], preferred_element_type=f32).astype(bf16)
+        if dest is p:
+            pr[p] = made
+        else:
+            po[dest] = made
+            final.append(send(po.at[dest], pr.at[p], fresh(), {"tp": dest}))
+    for copy in final:
+        copy.wait_recv()
+
+    @pl.loop(0, own // STEP)
+    def _(i):
+        rows = pl.ds(pl.multiple_of(i * STEP, STEP), STEP)
+        for j in range(4):
+            cols = slice(j * modw, (j + 1) * modw)
+            gate = mod[j, 4:5, :]
+            out_ref[rows, cols] = (
+                lat[p, rows, cols].astype(f32) + gate * pr[j, rows, :].astype(f32)
+            ).astype(bf16)
+
+    for copy in sends:
+        copy.wait_send()
+
+    @pl.when(has_right)
+    def _():
+        hop(z, z + 1, 0).wait_send()
+
+    @pl.when(has_left)
+    def _():
+        hop(z, z - 1, 1).wait_send()
+
+    for step in range(spn - 1):
+        left, right = z - 1 - step, z + 1 + step
+
+        @pl.when(left >= 0)
+        def _():
+            cross(left, core).wait_send()
+
+            @pl.when(has_right)
+            def _():
+                hop(left, z + 1, 0).wait_send()
+
+        @pl.when(right < spn)
+        def _():
+            cross(right, core).wait_send()
+
+            @pl.when(has_left)
+            def _():
+                hop(right, z - 1, 1).wait_send()
+
+
+def fused_device(
+    latents,
+    conditions,
+    context,
+    w_shift,
+    w_scale,
+    w_gate,
+    w_qdown,
+    w_kvdown,
+    w_rope,
+    q_gain,
+    latent_norm_gain,
+    query_up_weight,
+    key_up_weight,
+    value_up_weight,
+    context_bias,
+    w_out,
+):
+    f32, bf16 = jnp.float32, jnp.bfloat16
+    spn = lax.axis_size("sp")
+    own, width = latents.shape
+    ctxn = context.shape[0]
+    tok = 4 * own
+    seg = tok + ctxn
+    heads = context_bias.shape[0]
+    modw = w_shift.shape[1]
+    kdim, qcols = w_qdown.shape
+    kcols = w_kvdown.shape[1]
+    cosine, sine = turn_tables(tok * spn)
+    vmem = pl.BlockSpec(memory_space=pltpu.VMEM)
+    smem = pl.BlockSpec(memory_space=pltpu.SMEM)
+    hbm = pl.BlockSpec(memory_space=pl.ANY)
+    V, DMA = pltpu.VMEM, pltpu.SemaphoreType.DMA
+    scratch = [
+        V((16, conditions.shape[1]), f32),
+        V((3,) + w_shift.shape, bf16),
+        V((4, own, width), bf16),
+        V((ctxn, width), bf16),
+        V((seg, width), bf16),
+        V((kdim, qcols), bf16),
+        V((kdim, kcols + 128), bf16),
+        V((spn, 8, modw), f32),
+        V((4, 8, modw), f32),
+        V((4, 2, 2 * own, qcols), bf16),
+        V((4, 2, 2 * own, kcols), bf16),
+        V((4, ctxn, kcols), bf16),
+        V((seg, 128), f32),
+        V((spn, 2, seg // 2 + STEP, 4 * kcols), bf16),
+        V((tok, 4 * qcols), bf16),
+        V(query_up_weight.shape, bf16),
+        V(key_up_weight.shape, bf16),
+        V(value_up_weight.shape, bf16),
+        V(w_out.shape, bf16),
+        V((tok, 128), f32),
+        V((tok, 128), f32),
+        V((heads, tok, 128), bf16),
+        V((heads, seg, 128), bf16),
+        V((heads, seg, 128), bf16),
+        V((heads, tok, 128), f32),
+        V((heads, tok, 128), f32),
+        V((4, heads // 2, tok, 128), bf16),
+        V((4, own, modw), bf16),
+        V((4, own, modw), bf16),
+        DMA((13,)),
+        DMA((48,)),
+        DMA((48,)),
+        DMA((2, spn)),
+        DMA((spn,)),
+        DMA((spn,)),
+        DMA((spn,)),
+    ]
+    return pl.pallas_call(
+        block_kernel,
+        out_shape=jax.ShapeDtypeStruct(latents.shape, bf16),
+        in_specs=[vmem, smem, vmem, vmem, vmem] + [hbm] * 13,
+        out_specs=vmem,
+        scratch_shapes=scratch,
+        compiler_params=pltpu.CompilerParams(
+            collective_id=0, has_side_effects=True, vmem_limit_bytes=60 * 1024 * 1024
+        ),
+    )(
+        conditions,
+        context_bias,
+        q_gain[None, :],
+        latent_norm_gain[None, :],
+        w_rope,
+        latents,
+        context,
+        w_shift,
+        w_scale,
+        w_gate,
+        w_qdown,
+        w_kvdown,
+        query_up_weight,
+        key_up_weight,
+        value_up_weight,
+        w_out,
+        jnp.asarray(cosine),
+        jnp.asarray(sine),
+    )
+
+
+def on_device(*arrays):
+    latents, context, bias = arrays[0], arrays[2], arrays[14]
+    fits = (
+        lax.axis_size("tp") == 4
+        and latents.shape[0] % 32 == 0
+        and context.shape[0] % 64 == 0
+        and (4 * latents.shape[0] + context.shape[0]) == 512
+        and arrays[6].shape[1] == 256
+        and arrays[7].shape[1] == 128
+        and bias.shape[0] == 8
+    )
+    return fused_device(*arrays) if fits else plain_device(*arrays)
+
+
 def solution(mesh):
     in_specs = (
         P(("grp", "sp", "tp"), None),

time: 226 us -> 103 us (0.46)
  Pallas kernels: 0 us -> 98.7 us
  blocking collectives: 85.3 us -> 0 us
  waiting for transfers between devices: 58.1 us -> 0 us
  matrix products: 49 us -> 0 us
  other arithmetic: 16.1 us -> 0 us
  between operations: 13.5 us -> 0.01 us
    pallas_call x0 -> x1, Pallas kernels: none -> 98.7 us  [fused_device(): pl.pallas_call(block_kernel, out_shape=jax.ShapeDtypeStruct(latents.shape...]
    all_gather x3 -> x0, waiting for transfers between devices: 58 us -> none  [the longest x1 32.7 us: on_device(): arrived = lax.all_gather(h_own, 'tp', axis=0, tiled=True)]
    all_gather x7 -> x0, blocking collectives: 50.5 us -> none  [the longest x1 14.7 us: on_device(): lax.all_gather(kr_all, 'sp', axis=0, tiled=True)]
    dot_general x28 -> x0, matrix products: 49 us -> none  [the longest x4 7.78 us: attend_block(): jnp.einsum('ihd,jhd->ihj', q_nope, key_block, preferred_element_type=jnp....]
    psum x1 -> x0, blocking collectives: 20.8 us -> none  [on_device(): summed = lax.psum(partial_mod, 'sp')]
    all_to_all x1 -> x0, blocking collectives: 14 us -> none  [on_device(): lax.all_to_all(proj_cols.astype(jnp.bfloat16), 'tp', split_axis=0, concat...]
    reduce_sum x11 -> x0, other arithmetic: 9.36 us -> none  [the longest x4 3.35 us: attend_block(): running_sum = running_sum * rescale + jnp.sum(exponent, axis=-1)]
    convert_element_type x10 -> x0, other arithmetic: 3.7 us -> none  [the longest x2 1.47 us: layer_modulate(): return (normed * (1.0 + scale_by) + shift_by).astype(jnp.bfloat16)]
  transfers between devices with their start and end apart: 3 -> 0, of which waited for: 3 -> 0; matrix products, arithmetic and copies ran while one was open for 4% -> 0% of each run, Pallas kernels for 0% -> 0%
where the time goes in v1:
time: 103 us
  Pallas kernels  98.7 us (96%)
  local copies, waits for them, and re-layouts  4.35 us (4%)
    pallas_call x1, Pallas kernels, fused_device(): pl.pallas_call(block_kernel, out_shape=jax.ShapeDtypeStruct(latents.shape...  98.7 us
    unnamed x2, local copies, waits for them, and re-layouts  4.35 us

profile of v1, /device:TPU:0, one launch (start us, length us, event | category | flops | bytes accessed | tf_op | source)
XLA Modules:
  0.0 103.1 jit_solution(18120364221873081217)
XLA Ops:
  0.0 2.3 %copy.19.rope_ref = bf16[4096,32]{1,0:T(8,128)(2,1)} copy(bf16[4096,32]{0,1:T(8,128)(2,1)} %param.26) | data formatting | bytes 524288 | tf_op args[8]
  2.3 98.7 %shard_map.172 = bf16[96,4096]{1,0:T(8,128)(2,1)} custom-call(f32[2,1024]{1,0:T(2,128)} %cond_ref.1, f32[8]{0:T(128)} %bias_ref.1, f32[1,1024]{1,0:T(1,128)} %bitcast.2, f32[1,512]{1,0:T(1,128)} %bitcast.3, bf16[4096,32]{1,0:T(8,128)(2,1)} %copy.19.rope_ref, bf16[96,4096]{1,0:T(8,128)(2,1)} %lat_hbm.1, bf16[128,4096]{1,0:T(8,128)(2,1)} %ctx_hbm.1, ...), custom_call_target="tpu_custom_call" | custom-call | tf_op jit(solution)/shard_map/pallas_call | solution.py:811
  101.0 2.1 %copy.21 = bf16[96,4096]{1,0:T(8,128)(2,1)} copy(bf16[96,4096]{1,0:T(8,128)(2,1)} %shard_map.172) | data formatting | bytes 1572864

commit v2 on v1

--- a/solution.py
+++ b/solution.py
@@ -207,6 +207,7 @@
 MESH = pl.DeviceIdType.MESH
 LOG2E = 1.4426950408889634
 STEP = 16
+BAND = 32
 
 
 def turn_tables(tokens):
@@ -288,6 +289,9 @@
     att,
     po,
     pr,
+    st_mean,
+    st_rate,
+    part,
     load_sem,
     send_sem,
     recv_sem,
@@ -388,28 +392,74 @@
     act = (conditions / (1.0 + jnp.exp(-conditions))).astype(bf16)
 
     pl.semaphore_wait(barrier, 3 + spn - 1)
+    def near(view):
+        return send(view(p), view(p), fresh(), {"tp": p1}).wait_recv
+
+    def far(view):
+        i2, i3 = fresh(), fresh()
+        first = send(view(p), view(p), i2, {"tp": p2})
+
+        def relay():
+            first.wait_recv()
+            return send(view(p2), view(p2), i3, {"tp": p1}).wait_recv
+
+        return relay
+
     l_lat.wait()
-    half_own = own // 2
-    relay_lat = []
-    lat_near = []
-    for piece in range(2):
-        rows = pl.ds(piece * half_own, half_own)
-        r, w = spread(lambda slot, rows=rows: lat.at[slot, rows])
-        relay_lat.append(r)
-        lat_near.append(w)
+    lat_near = near(lambda slot: lat.at[slot])
+    lat_rows = [slice(r, r + BAND) for r in range(0, own, BAND)]
+    lat_views = [lambda slot, r=r: lat.at[slot, pl.ds(r.start, BAND)] for r in lat_rows]
+    lat_relay = [far(lat_views[0])]
 
     for i in range(3):
         l_w3[i].wait()
-        part = jnp.dot(act, w3[i], preferred_element_type=f32)
-        modp[z, 2 * i : 2 * i + 2, :] = part[0:2]
+        partial_mod = jnp.dot(act, w3[i], preferred_element_type=f32)
+        modp[z, 2 * i : 2 * i + 2, :] = partial_mod[0:2]
     modp[z, 6:8, :] = jnp.zeros((2, modw), f32)
     mod_waits = []
     for d in range(1, spn):
         mod_waits.append(
             send(modp.at[z], modp.at[z], fresh(), {"sp": lax.rem(z + d, spn)})
         )
-    wkvr[:, kcols:] = jnp.zeros((width, wkvr.shape[1] - kcols), bf16)
+    wkvr[:, kcols + ROTARY_DIM :] = jnp.zeros((width, wkvr.shape[1] - kcols - ROTARY_DIM), bf16)
     wkvr[:, kcols : kcols + ROTARY_DIM] = rope_ref[...]
+
+    def measured(src, row_count, dst_row):
+        @pl.loop(0, row_count // BAND)
+        def _(i):
+            rows = pl.ds(pl.multiple_of(i * BAND, BAND), BAND)
+            to = pl.ds(pl.multiple_of(dst_row + i * BAND, BAND), BAND)
+            tiles = [slice(c, c + 128) for c in range(0, width, 128)]
+            sums = jnp.zeros((BAND, 128), f32)
+            for c in tiles:
+                sums = sums + src[rows, c].astype(f32)
+            mean = jnp.broadcast_to(
+                jnp.sum(sums, axis=-1, keepdims=True) * (1.0 / width), (BAND, 128)
+            )
+            squares = jnp.zeros((BAND, 128), f32)
+            for c in tiles:
+                center = src[rows, c].astype(f32) - mean
+                squares = squares + center * center
+            spread_of = jnp.sum(squares, axis=-1, keepdims=True) * (1.0 / width)
+            st_mean[to, :] = mean
+            st_rate[to, :] = jnp.broadcast_to(lax.rsqrt(spread_of + EPSILON), (BAND, 128))
+
+    def modulate(src, row_count, dst_row, which):
+        @pl.loop(0, row_count // BAND)
+        def _(i):
+            rows = pl.ds(pl.multiple_of(i * BAND, BAND), BAND)
+            to = pl.ds(pl.multiple_of(dst_row + i * BAND, BAND), BAND)
+            mean, rate = st_mean[to, :], st_rate[to, :]
+            for c in range(0, width, 128):
+                j, k = c // modw, c % modw
+                shift_by = mod[j, which : which + 1, k : k + 128]
+                scale_by = mod[j, 2 + which : 3 + which, k : k + 128]
+                normed = (src[rows, c : c + 128].astype(f32) - mean) * rate
+                hid[to, c : c + 128] = (normed * (1.0 + scale_by) + shift_by).astype(bf16)
+
+    measured(lat.at[p], own, p * own)
+    l_ctx.wait()
+    measured(ctx, ctxn, tok)
     for copy in mod_waits:
         copy.wait_recv()
     total = modp[0]
@@ -417,26 +467,14 @@
         total = total + modp[i]
     mod[p] = total
     mod_waits = [send(mod.at[p], mod.at[p], fresh(), {"tp": peer}) for peer in (p2, p3, p1)]
-    lat_far = [relay_lat[0]()]
+    for view in lat_views[1:]:
+        lat_relay.append(far(view))
+    lat_near()
+    measured(lat.at[p1], own, p1 * own)
+    lat_far = [lat_relay[0]()]
     for copy in mod_waits:
         copy.wait_recv()
 
-    def modulate(src, row_count, dst_row, which):
-        @pl.loop(0, row_count // STEP)
-        def _(i):
-            rows = pl.ds(pl.multiple_of(i * STEP, STEP), STEP)
-            values = src[rows, :].astype(f32)
-            center = values - jnp.mean(values, axis=-1, keepdims=True)
-            spread_of = jnp.mean(center * center, axis=-1, keepdims=True)
-            normed = center * lax.rsqrt(spread_of + EPSILON)
-            to = pl.ds(pl.multiple_of(dst_row + i * STEP, STEP), STEP)
-            for j in range(4):
-                shift_by = mod[j, which : which + 1, :]
-                scale_by = mod[j, 2 + which : 3 + which, :]
-                cols = slice(j * modw, (j + 1) * modw)
-                hid[to, cols] = (normed[:, cols] * (1.0 + scale_by) + shift_by).astype(bf16)
-
-    l_ctx.wait()
     modulate(ctx, ctxn, tok, 1)
     l_kd.wait()
     l_qd.wait()
@@ -446,8 +484,6 @@
     relays = [spread(lambda slot: kvc.at[slot])]
 
     modulate(lat.at[p], own, p * own, 0)
-    for w in lat_near:
-        w()
     modulate(lat.at[p1], own, p1 * own, 0)
 
     def down(half):
@@ -460,18 +496,24 @@
         return one, spread(lambda slot: cq.at[slot, half], lambda slot: cq.at[slot, 1 - half])
 
     kv_a, cq_a = down(side)
-    lat_far.append(relay_lat[1]())
-    modulate(lat.at[p2], own, p2 * own, 0)
-    for w in lat_far:
-        w()
-    modulate(lat.at[p3], own, p3 * own, 0)
+    for n, r in enumerate(lat_rows):
+        if n:
+            lat_far.append(lat_relay[n]())
+        piece = lat.at[p2, pl.ds(r.start, BAND)]
+        measured(piece, BAND, p2 * own + r.start)
+        modulate(piece, BAND, p2 * own + r.start, 0)
+    for n, r in enumerate(lat_rows):
+        lat_far[n]()
+        piece = lat.at[p3, pl.ds(r.start, BAND)]
+        measured(piece, BAND, p3 * own + r.start)
+        modulate(piece, BAND, p3 * own + r.start, 0)
     kv_b, cq_b = down(1 - side)
     relays += [kv_a, kv_b]
-    far = [r() for r, _ in relays]
-    for w in far:
+    kv_far = [r() for r, _ in relays]
+    for w in kv_far:
         w()
-    for _, near in relays:
-        near()
+    for _, w in relays:
+        w()
 
     l_cos.wait()
     l_sin.wait()
@@ -626,23 +668,31 @@
                     lane_h < 64, pltpu.roll(v2, 64, 1), ones
                 ).astype(bf16)
 
-    def attend(h):
-        scores = lax.dot_general(
+    def score(h):
+        return lax.dot_general(
             qh[h], kb[h], (((1,), (1,)), ((), ())), preferred_element_type=f32
         )
-        lat_s = scores[:, :tok] * factor
-        ctx_s = scores[:, tok:] * factor + bias_ref[h] * LOG2E
+
+    def attend(h, scores):
+        tiles = [scores[:, c : c + 128] * factor for c in range(0, seg, 128)]
+        bias = bias_ref[h] * LOG2E
+        tiles = [t + bias if n * 128 >= tok else t for n, t in enumerate(tiles)]
+        best = functools.reduce(jnp.maximum, tiles)
         old = mx[h]
-        best = jnp.maximum(
-            jnp.max(lat_s, axis=-1, keepdims=True), jnp.max(ctx_s, axis=-1, keepdims=True)
-        )
-        new = jnp.maximum(old, best)
+        new = jnp.maximum(old, jnp.max(best, axis=-1, keepdims=True))
         mx[h] = new
-        top = new[:, 0:1]
-        weights = jnp.concatenate([jnp.exp2(lat_s - top), jnp.exp2(ctx_s - top)], axis=1)
+        weights = jnp.concatenate([jnp.exp2(t - new).astype(bf16) for t in tiles], axis=1)
         acc[h] = acc[h] * jnp.exp2(old - new) + jnp.dot(
-            weights.astype(bf16), vb[h], preferred_element_type=f32
-        )
+            weights, vb[h], preferred_element_type=f32
+        )
+
+    def attend_all(after):
+        scores = score(0)
+        for h in range(heads):
+            following = score(h + 1) if h + 1 < heads else None
+            attend(h, scores)
+            after(h)
+            scores = following
 
     def block_at(step):
         below = jnp.minimum(z, spn - 1 - z)
@@ -650,7 +700,7 @@
         past = jnp.where(z < spn - 1 - z, step, spn - 1 - step)
         return jnp.where(step <= 2 * below, near, past)
 
-    @pl.loop(0, spn)
+    @pl.loop(0, spn - 1)
     def _(step):
         @pl.when(step > 0)
         def _():
@@ -663,31 +713,52 @@
             cross(block, 1 - core).wait_recv()
 
         expand(block)
-        for h in range(heads):
-            attend(h)
-
-    att_relays = []
+        attend_all(lambda h: None)
+
+    att_relay, att_near = [], []
     lane64 = lane < 64
-    for hp in range(heads // 2):
+
+    def finish(h):
+        if h % 2 == 0:
+            return
+        hp = h // 2
         outs = []
-        for h in (2 * hp, 2 * hp + 1):
-            a = acc[h]
+        for g in (h - 1, h):
+            a = acc[g]
             outs.append(a / a[:, VALUE_DIM : VALUE_DIM + 1])
         att[p, hp] = jnp.where(lane64, outs[0], pltpu.roll(outs[1], 64, 1)).astype(bf16)
-        att_relays.append(spread(lambda slot, hp=hp: att.at[slot, hp]))
-    att_far = [r() for r, _ in att_relays]
+        att_relay.append(far(lambda slot: att.at[slot, hp]))
+        att_near.append(near(lambda slot: att.at[slot, hp]))
+
+    arrive(spn - 2)
+    last_block = block_at(jnp.int32(spn - 1))
+    cross(last_block, 1 - core).wait_recv()
+    expand(last_block)
+    attend_all(finish)
+
+    l_wo.wait()
+    half_k = heads * VALUE_DIM * 2
+    order = (p2, p3, p1, p)
+
+    def project(dest, chip):
+        rows = pl.ds(pl.multiple_of(dest * own, STEP), own)
+        joined = jnp.concatenate(
+            [att[2 * chip + r, hp, rows, :] for r in range(2) for hp in range(heads // 2)], axis=1
+        )
+        k_rows = pl.ds(pl.multiple_of(chip * half_k, 128), half_k)
+        return jnp.dot(joined, wo[k_rows, :], preferred_element_type=f32)
+
+    att_far = [att_relay[0](), att_relay[1]()]
+    for w in att_near:
+        w()
+    for dest in order:
+        part[dest] = project(dest, side)
+    att_far += [r() for r in att_relay[2:]]
     for w in att_far:
         w()
-    for _, near in att_relays:
-        near()
-    l_wo.wait()
     final = []
-    for dest in (p2, p3, p1, p):
-        rows = pl.ds(pl.multiple_of(dest * own, STEP), own)
-        joined = jnp.concatenate(
-            [att[r, hp, rows, :] for r in range(4) for hp in range(heads // 2)], axis=1
-        )
-        made = jnp.dot(joined, wo[...], preferred_element_type=f32).astype(bf16)
+    for dest in order:
+        made = (part[dest] + project(dest, 1 - side)).astype(bf16)
         if dest is p:
             pr[p] = made
         else:
@@ -800,6 +871,9 @@
         V((4, heads // 2, tok, 128), bf16),
         V((4, own, modw), bf16),
         V((4, own, modw), bf16),
+        V((seg, 128), f32),
+        V((seg, 128), f32),
+        V((4, own, modw), f32),
         DMA((13,)),
         DMA((48,)),
         DMA((48,)),

time: 103 us -> 88.2 us (0.86)
  Pallas kernels: 98.7 us -> 83.5 us
    pallas_call x1, Pallas kernels: 98.7 us -> 83.5 us  [fused_device(): pl.pallas_call(block_kernel, out_shape=jax.ShapeDtypeStruct(latents.shape...]
where the time goes in v2:
time: 88.2 us; the launch traced here: 87.8 us
  Pallas kernels  83.5 us (95%)
  local copies, waits for them, and re-layouts  4.35 us (5%)
    pallas_call x1, Pallas kernels, fused_device(): pl.pallas_call(block_kernel, out_shape=jax.ShapeDtypeStruct(latents.shape...  83.5 us
    unnamed x2, local copies, waits for them, and re-layouts  4.35 us

profile of v2, /device:TPU:0, one launch (start us, length us, event | category | flops | bytes accessed | tf_op | source)
XLA Modules:
  0.0 87.8 jit_solution(1170116792326245436)
XLA Ops:
  0.0 2.3 %copy.19.rope_ref = bf16[4096,32]{1,0:T(8,128)(2,1)} copy(bf16[4096,32]{0,1:T(8,128)(2,1)} %param.26) | data formatting | bytes 524288 | tf_op args[8]
  2.3 83.5 %shard_map.172 = bf16[96,4096]{1,0:T(8,128)(2,1)} custom-call(f32[2,1024]{1,0:T(2,128)} %cond_ref.1, f32[8]{0:T(128)} %bias_ref.1, f32[1,1024]{1,0:T(1,128)} %bitcast.2, f32[1,512]{1,0:T(1,128)} %bitcast.3, bf16[4096,32]{1,0:T(8,128)(2,1)} %copy.19.rope_ref, bf16[96,4096]{1,0:T(8,128)(2,1)} %lat_hbm.1, bf16[128,4096]{1,0:T(8,128)(2,1)} %ctx_hbm.1, ...), custom_call_target="tpu_custom_call" | custom-call | tf_op jit(solution)/shard_map/pallas_call | solution.py:885
  85.8 2.1 %copy.21 = bf16[96,4096]{1,0:T(8,128)(2,1)} copy(bf16[96,4096]{1,0:T(8,128)(2,1)} %shard_map.172) | data formatting | bytes 1572864
